TPU v7x, 256 devices: a whole 4x4x8 slice. The times are simulated.
256 devices in a mesh: ep: 128 (over z, y, x), tp: 2 (over core).
Axes of the slice: x: 4, y: 4, z: 8, core: 2. Of those that a mesh axis runs over, the one named last changes fastest.
Arguments:
- tokens: bfloat16 [512, 2048], P('ep'), may hold values from -6 to 6
- lengths: int32 [512], P('ep'), may hold values from 1 to 1024
- cache_keys: bfloat16 [512, 1024, 512], P('ep', None, 'tp'), may hold values from -640 to 640
- cache_values: bfloat16 [512, 1024, 512], P('ep', None, 'tp'), may hold values from -6 to 6
- norm0_gain: float32 [2048], replicated, may hold values from 0.1 to 1.9
- query_weight: bfloat16 [2048, 1536], P('ep', 'tp'), may hold values from -0.125 to 0.125
- key_weight: bfloat16 [2048, 512], P('ep', 'tp'), may hold values from -0.21875 to 0.21875
- value_weight: bfloat16 [2048, 512], P('ep', 'tp'), may hold values from -0.125 to 0.125
- mix_lambda: float32 [6], P('tp'), may hold values from 0.3 to 0.8
- head_gain: float32 [256], replicated, may hold values from 0.1 to 1.9
- out_weight: bfloat16 [1536, 2048], P('tp', 'ep'), may hold values from -0.15625 to 0.15625
- norm1_gain: float32 [2048], replicated, may hold values from 0.1 to 1.9
- group_ids: int32 [512], P('ep'), may hold values from 0 to 31, as said below
- member_ids: int32 [512, 2], P('ep'), may hold values from 0 to 3, as said below
- group_weight: float32 [512], P('ep'), may hold values from 0.3 to 1
- member_weights: float32 [512, 2], P('ep'), may hold values from 0.2 to 1
- expert_gate: bfloat16 [128, 2048, 512], P('ep', None, 'tp'), may hold values from -0.125 to 0.125
- expert_up: bfloat16 [128, 2048, 512], P('ep', None, 'tp'), may hold values from -0.125 to 0.125
- expert_down: bfloat16 [128, 512, 2048], P('ep', 'tp'), may hold values from -0.25 to 0.25
- norm2_gain: float32 [2048], P('tp'), may hold values from 0.1 to 1.9
Outputs:
- result: bfloat16 [512, 2048], P('ep', 'tp')
Inputs may be any that keep to these rules, and one draw needn't show every extreme that they name: `group_ids`: every group is named by exactly 16 tokens; the 4 tokens of one device name different groups. `member_ids`: A token's 2 members are different; no expert is used by more than 16 tokens, and some expert by exactly 16.
All inputs are finite; a program needn't handle non-finite values.
Results may differ from a plain program's by a relative error of at most 0.015.
Values may be sent and summed in bfloat16 or wider, within the bound.
No kernel may reach another device: no remote copies, remote signals or barrier semaphores. Data moves between devices by JAX's collectives and lax.ppermute only.
A program may use at most 64 MiB of HBM per device.

v0:
```python
import jax
import jax.numpy as jnp
from jax import lax
from jax.sharding import Mesh
from jax.sharding import PartitionSpec as P

EPG = 4
EP = ("z", "y", "x")
ROW = ("y", "x")
ALPHA = 2.0**0.25
EPS = 1e-05


def swap(array, axis):
    return lax.all_to_all(array, axis, 0, 0, tiled=True)


def to_all(array, axis):
    return swap(jnp.broadcast_to(array[None], (lax.axis_size(axis), *array.shape)), axis)


def layer_norm(values, gain):
    mean = jnp.mean(values, -1, keepdims=True)
    spread = jnp.mean(jnp.square(values - mean), -1, keepdims=True)
    return (values - mean) * lax.rsqrt(spread + EPS) * gain


def attend(queries, new_keys, new_values, cache_keys, cache_values, lengths, mix_lambda, head_gain):
    seqs = queries.shape[0]
    span = cache_keys.shape[1]
    vwidth = head_gain.shape[0]
    kv_local = cache_values.shape[2] // vwidth
    hwidth = cache_keys.shape[2] // (2 * kv_local)
    heads_local = mix_lambda.shape[0]
    group = heads_local // kv_local
    query_grid = queries.reshape(seqs, kv_local, group, 2, hwidth)
    cached_keys = cache_keys.reshape(seqs, span, kv_local, 2, hwidth)
    fresh_keys = new_keys.reshape(seqs, kv_local, 2, hwidth)
    cached_values = cache_values.reshape(seqs, span, kv_local, vwidth)
    fresh_values = new_values.reshape(seqs, kv_local, vwidth)
    valid = (jnp.arange(span, dtype=jnp.int32)[None, :] < lengths[:, None])[:, None, None, :]
    scale = hwidth ** (-0.5)
    maps = []
    for which in range(2):
        cached = (
            jnp.einsum(
                "sghd,scgd->sghc",
                query_grid[:, :, :, which],
                cached_keys[:, :, :, which],
                preferred_element_type=jnp.float32,
            )
            * scale
        )
        fresh = (
            jnp.einsum(
                "sghd,sgd->sgh",
                query_grid[:, :, :, which],
                fresh_keys[:, :, which],
                preferred_element_type=jnp.float32,
            )
            * scale
        )
        highest = jnp.maximum(jnp.max(jnp.where(valid, cached, -1e30), -1), fresh)
        spread = jnp.where(valid, jnp.exp(cached - highest[..., None]), 0.0)
        itself = jnp.exp(fresh - highest)
        total = jnp.sum(spread, -1) + itself
        maps.append((spread / total[..., None], itself / total))
    lambdas = mix_lambda.reshape(1, kv_local, group)
    cached_weight = (maps[0][0] - lambdas[..., None] * maps[1][0]).astype(jnp.bfloat16)
    fresh_weight = (maps[0][1] - lambdas * maps[1][1]).astype(jnp.bfloat16)
    head_out = jnp.einsum(
        "sghc,scgv->sghv", cached_weight, cached_values, preferred_element_type=jnp.float32
    )
    head_out = (
        head_out
        + fresh_weight.astype(jnp.float32)[..., None]
        * fresh_values.astype(jnp.float32)[:, :, None, :]
    )
    head_out = (
        head_out * lax.rsqrt(jnp.mean(head_out * head_out, -1, keepdims=True) + EPS) * head_gain
    )
    return head_out.astype(jnp.bfloat16).reshape(seqs, heads_local * vwidth)


def shards(
    tokens,
    lengths,
    cache_keys,
    cache_values,
    norm0_gain,
    query_weight,
    key_weight,
    value_weight,
    mix_lambda,
    head_gain,
    out_weight,
    norm1_gain,
    group_ids,
    member_ids,
    group_weight,
    member_weights,
    expert_gate,
    expert_up,
    expert_down,
    norm2_gain,
):
    seqs, width = tokens.shape
    deep = lax.axis_size("z")
    experts = lax.axis_size(EP)
    halves = lax.axis_size("tp")
    half = width // halves
    block = width // deep
    query_cols = query_weight.shape[1]
    key_cols = key_weight.shape[1]
    value_cols = value_weight.shape[1]
    proj_cols = query_cols + key_cols + value_cols
    expert_ids = group_ids[:, None] * EPG + member_ids
    share = group_weight[:, None] * member_weights
    own_weights = jnp.concatenate((query_weight, key_weight, value_weight, out_weight.T), 1)
    weights = to_all(own_weights, ROW).reshape(block, -1)
    weight_in = weights[:, :proj_cols]
    weight_out = weights[:, proj_cols:]
    normed = layer_norm(tokens.astype(jnp.float32), norm0_gain).astype(jnp.bfloat16)
    columns = swap(normed.reshape(seqs, deep, block).transpose(1, 0, 2), "z")
    partial = jnp.dot(
        columns.reshape(deep * seqs, block), weight_in, preferred_element_type=jnp.float32
    )
    projected = jnp.sum(swap(partial.reshape(deep, seqs, proj_cols), "z"), 0).astype(jnp.bfloat16)
    queries = projected[:, :query_cols]
    new_keys = projected[:, query_cols : query_cols + key_cols]
    new_values = projected[:, query_cols + key_cols :]
    attended = attend(
        queries, new_keys, new_values, cache_keys, cache_values, lengths, mix_lambda, head_gain
    )
    everyone = to_all(attended, "z").reshape(deep * seqs, -1)
    partial_mix = lax.dot_general(
        everyone, weight_out, (((1,), (1,)), ((), ())), preferred_element_type=jnp.float32
    ).astype(jnp.bfloat16)
    doubled = jnp.broadcast_to(
        partial_mix.reshape(deep, 1, seqs, block), (deep, halves, seqs, block)
    )
    back = swap(doubled.reshape(deep * halves, seqs, block), ("z", "tp"))
    mix = jnp.sum(back.astype(jnp.float32).reshape(deep, halves, seqs, block), 1)
    mix = mix.transpose(1, 0, 2).reshape(seqs, width).astype(jnp.bfloat16)
    stream = (ALPHA * normed.astype(jnp.float32) + mix.astype(jnp.float32)).astype(jnp.bfloat16)
    settled = layer_norm(stream.astype(jnp.float32), norm1_gain).astype(jnp.bfloat16)
    targets = lax.iota(jnp.int32, experts)
    select = jnp.any(expert_ids[None, :, :] == targets[:, None, None], 2)
    tiles = settled.reshape(1, seqs, width // 128, 128)
    sending = jnp.sum(
        jnp.where(select[:, :, None, None], tiles, jnp.zeros_like(tiles)).astype(jnp.float32), 1
    ).astype(jnp.bfloat16)
    rows = swap(sending, EP).reshape(experts, width)
    gate = jnp.dot(rows, expert_gate[0], preferred_element_type=jnp.float32)
    upward = jnp.dot(rows, expert_up[0], preferred_element_type=jnp.float32)
    hidden = (jax.nn.silu(gate) * upward).astype(jnp.bfloat16)
    output = jnp.dot(hidden, expert_down[0], preferred_element_type=jnp.float32)
    output = output.astype(jnp.bfloat16).reshape(experts * halves, half // 128, 128)
    returned = swap(output, EP + ("tp",)).reshape(experts, halves, half // 128, 128)
    both = jnp.sum(returned.astype(jnp.float32), 1)
    combine = jnp.sum(
        jnp.where(expert_ids[:, :, None] == targets[None, None, :], share[:, :, None], 0.0), 1
    )
    routed = jnp.sum(combine[:, :, None, None] * both[None], 1).reshape(seqs, half)
    own = lax.dynamic_slice_in_dim(settled, lax.axis_index("tp") * half, half, 1)
    mixed = ALPHA * own.astype(jnp.float32) + routed
    sums = lax.psum(jnp.stack((jnp.sum(mixed, 1), jnp.sum(mixed * mixed, 1))), "tp")
    mean = sums[0] / width
    spread = sums[1] / width - mean * mean
    result = (mixed - mean[:, None]) * lax.rsqrt(spread[:, None] + EPS) * norm2_gain
    return result.astype(jnp.bfloat16)


def solution(mesh):
    torus = Mesh(mesh.devices.reshape(8, 4, 4, mesh.shape["tp"]), ("z", "y", "x", "tp"))
    return jax.shard_map(
        shards,
        mesh=torus,
        in_specs=(
            P(EP, None),
            P(EP),
            P(EP, None, "tp"),
            P(EP, None, "tp"),
            P(),
            P(EP, "tp"),
            P(EP, "tp"),
            P(EP, "tp"),
            P("tp"),
            P(),
            P("tp", EP),
            P(),
            P(EP),
            P(EP, None),
            P(EP),
            P(EP, None),
            P(EP, None, "tp"),
            P(EP, None, "tp"),
            P(EP, "tp", None),
            P("tp"),
        ),
        out_specs=P(EP, "tp"),
        check_vma=False,
    )
```

profile of v0, /device:TPU:1, one launch (start us, length us, event | category | flops | bytes accessed | tf_op | source)
XLA Modules:
  0.0 149.5 jit_solution(3451434910616258476)
XLA Ops:
  0.0 1.0 convert_reduce_fusion.2
  1.0 0.9 fusion.31
  1.9 1.4 fusion.33
  3.3 9.0 %all-to-all-start = ((bf16[8,4,256]{2,1,0:T(4,128)(2,1)}), bf16[8,4,256]{2,1,0:T(4,128)(2,1)S(1)}, u32[]{:S(2)}, u32[]{:S(2)}) async-start(bf16[8,4,256]{2,1,0:T(4,128)(2,1)} %bitcast.1), calls=%async_computation | async-start | bytes 32768 | tf_op jit(solution)/shard_map/all_to_all | solution.py:15
  13.1 5.8 %all-to-all-done = bf16[8,4,256]{2,1,0:T(4,128)(2,1)S(1)} async-done(((bf16[8,4,256]{2,1,0:T(4,128)(2,1)}), bf16[8,4,256]{2,1,0:T(4,128)(2,1)S(1)}, u32[]{:S(2)}, u32[]{:S(2)}) %all-to-all-start) | async-done | bytes 16416 | tf_op jit(solution)/shard_map/all_to_all | solution.py:15
  19.1 22.2 %all_to_all.35 = bf16[16,16,2048]{2,1,0:T(8,128)(2,1)S(1)} all-to-all(bf16[16,16,2048]{2,1,0:T(8,128)(2,1)S(1)} %broadcast_in_dim.116), channel_id=1, replica_groups=mesh['z'=8,'y'=4,'x'=4,'tp'=2] {'y','x'}, dimensions={0} | all-to-all | bytes 2097152 | tf_op jit(solution)/shard_map/all_to_all | solution.py:15
  41.3 0.9 fusion.6
  42.2 3.4 %all-to-all-start.2 = ((f32[8,4,1280]{2,1,0:T(4,128)}), f32[8,4,1280]{2,1,0:T(4,128)S(1)}, u32[]{:S(2)}, u32[]{:S(2)}) async-start(f32[8,4,1280]{2,1,0:T(4,128)} %fusion.6), calls=%async_computation.2 | async-start | bytes 327680 | tf_op jit(solution)/shard_map/all_to_all | solution.py:15
  45.6 4.0 %copy.53 = bf16[4,1024,256]{1,2,0:T(8,128)(2,1)} copy(bf16[4,1024,256]{2,1,0:T(8,128)(2,1)} %param.22) | data formatting | bytes 4194304 | tf_op args[2]
  49.7 4.1 %all-to-all-done.2 = f32[8,4,1280]{2,1,0:T(4,128)S(1)} async-done(((f32[8,4,1280]{2,1,0:T(4,128)}), f32[8,4,1280]{2,1,0:T(4,128)S(1)}, u32[]{:S(2)}, u32[]{:S(2)}) %all-to-all-start.2) | async-done | bytes 163872 | tf_op jit(solution)/shard_map/all_to_all | solution.py:15
  53.9 1.6 %select_reduce_fusion.2 = (f32[4,3]{1,0:T(4,128)S(1)}, f32[4,3,1024]{2,1,0:T(4,128)S(1)}) fusion(pred[4,1024]{1,0:T(4,128)(4,1)S(1)} %iota_compare_fusion, bf16[4,1024,1,2,128]{1,4,3,0,2:T(8,128)(2,1)} %bitcast.111, bf16[4,1,3,1,128]{4,0,3,2,1:T(4,128)(2,1)S(1)} %get-tuple-element.17), kind=kOutput, calls=%fused_computation.34 | convolution fusion | flops 3182580 | bytes 1104944 | tf_op jit(solution)/shard_map/sghd,scgd->sghc/dot_general | solution.py:46
  55.6 1.6 %fusion.21 = (f32[4,3]{1,0:T(4,128)S(1)}, f32[4,3]{1,0:T(4,128)S(1)}, f32[4,3,1024]{2,1,0:T(4,128)S(1)}) fusion(f32[4,3,1024]{2,1,0:T(4,128)S(1)} %get-tuple-element.21, f32[4,3]{1,0:T(4,128)S(1)} %multiply_maximum_fusion.1, pred[4,1024]{1,0:T(4,128)(4,1)S(1)} %iota_compare_fusion, bf16[4,1024,1,2,128]{1,4,3,0,2:T(8,128)(2,1)} %bitcast.112, ...), kind=kOutput, calls=%fused_computation.36 | convolution fusion | flops 3219432 | bytes 1154192 | tf_op jit(solution)/shard_map/sghd,scgd->sghc/dot_general | solution.py:46
  58.7 3.3 %all-to-all-start.3 = ((bf16[8,4,768]{2,1,0:T(4,128)(2,1)}), bf16[8,4,768]{2,1,0:T(4,128)(2,1)S(1)}, u32[]{:S(2)}, u32[]{:S(2)}) async-start(bf16[8,4,768]{2,1,0:T(4,128)(2,1)} %broadcast_in_dim.120), calls=%async_computation.3 | async-start | bytes 98304 | tf_op jit(solution)/shard_map/all_to_all | solution.py:15
  62.1 6.9 %all-to-all-done.3 = bf16[8,4,768]{2,1,0:T(4,128)(2,1)S(1)} async-done(((bf16[8,4,768]{2,1,0:T(4,128)(2,1)}), bf16[8,4,768]{2,1,0:T(4,128)(2,1)S(1)}, u32[]{:S(2)}, u32[]{:S(2)}) %all-to-all-start.3) | async-done | bytes 49184 | tf_op jit(solution)/shard_map/all_to_all | solution.py:15
  70.0 8.5 %all-to-all-start.4 = ((bf16[16,4,256]{2,1,0:T(4,128)(2,1)}), bf16[16,4,256]{2,1,0:T(4,128)(2,1)S(1)}, u32[]{:S(2)}, u32[]{:S(2)}) async-start(bf16[16,4,256]{2,1,0:T(4,128)(2,1)} %bitcast.20), calls=%async_computation.4 | async-start | bytes 65536 | tf_op jit(solution)/shard_map/all_to_all | solution.py:15
  78.7 7.3 %all-to-all-done.4 = bf16[16,4,256]{2,1,0:T(4,128)(2,1)S(1)} async-done(((bf16[16,4,256]{2,1,0:T(4,128)(2,1)}), bf16[16,4,256]{2,1,0:T(4,128)(2,1)S(1)}, u32[]{:S(2)}, u32[]{:S(2)}) %all-to-all-start.4) | async-done | bytes 32800 | tf_op jit(solution)/shard_map/all_to_all | solution.py:15
  86.6 1.0 select_reduce_fusion
  87.6 24.7 %all_to_all.36 = bf16[128,16,128]{2,1,0:T(8,128)(2,1)S(1)} all-to-all(bf16[128,16,128]{2,1,0:T(8,128)(2,1)S(1)} %select_reduce_fusion), channel_id=1, replica_groups=mesh['z'=8,'y'=4,'x'=4,'tp'=2] {'z','y','x'}, dimensions={0} | all-to-all | bytes 1048576 | tf_op jit(solution)/shard_map/all_to_all | solution.py:15
  112.3 1.5 %fusion.4 = f32[128,256]{1,0:T(8,128)S(1)} fusion(bf16[1,2048,256]{2,1,0:T(8,128)(2,1)} %param.36, bf16[16,8,16,128]{3,2,1,0:T(8,128)(2,1)S(1)} %bitcast.107), kind=kOutput, calls=%fused_computation.14 | convolution fusion | flops 134217728 | bytes 1703936 | tf_op jit(solution)/shard_map/dot_general | solution.py:154
  113.8 2.3 %convolution_convert_fusion = bf16[128,2048]{1,0:T(8,128)(2,1)S(1)} fusion(bf16[1,256,2048]{2,1,0:T(8,128)(2,1)} %param.38, bf16[1,2048,256]{2,1,0:T(8,128)(2,1)} %param.37, bf16[16,8,16,128]{3,2,1,0:T(8,128)(2,1)S(1)} %bitcast.108, f32[128,256]{1,0:T(8,128)S(1)} %fusion.4), kind=kOutput, calls=%fused_computation | convolution fusion | flops 268894208 | bytes 3276800 | tf_op jit(solution)/shard_map/dot_general | solution.py:157
  116.2 1.0 reshape.284
  117.2 7.5 %all-to-all-start.6 = ((bf16[256,8,128]{2,1,0:T(8,128)(2,1)}), bf16[256,8,128]{2,1,0:T(8,128)(2,1)S(1)}, u32[]{:S(2)}, u32[]{:S(2)}) async-start(bf16[256,8,128]{2,1,0:T(8,128)(2,1)} %reshape.284), calls=%async_computation.6 | async-start | bytes 1048576 | tf_op jit(solution)/shard_map/all_to_all | solution.py:15
  124.9 19.8 %all-to-all-done.6 = bf16[256,8,128]{2,1,0:T(8,128)(2,1)S(1)} async-done(((bf16[256,8,128]{2,1,0:T(8,128)(2,1)}), bf16[256,8,128]{2,1,0:T(8,128)(2,1)S(1)}, u32[]{:S(2)}, u32[]{:S(2)}) %all-to-all-start.6) | async-done | bytes 524320 | tf_op jit(solution)/shard_map/all_to_all | solution.py:15
  145.8 3.0 %psum.7 = f32[2,4]{1,0:T(2,128)S(1)} all-reduce(f32[2,4]{1,0:T(2,128)S(1)} %pad_maximum_fusion.1), channel_id=1, replica_groups=mesh['z'=8,'y'=4,'x'=4,'tp'=2] {'tp'}, use_global_device_ids=true, to_apply=%region_18.19 | all-reduce | flops 8 | bytes 64 | tf_op jit(solution)/shard_map/psum | solution.py:167
  (72 shorter events, 6.4 us)
Async XLA Ops:
  0.0 57.4 %copy-start = (bf16[4,1024,256]{2,1,0:T(8,128)(2,1)S(1)}, bf16[4,1024,256]{2,1,0:T(8,128)(2,1)}, u32[]{:S(2)}) copy-start(bf16[4,1024,256]{2,1,0:T(8,128)(2,1)} %param.23) | copy-start | bytes 6291460
  3.3 15.6 %all-to-all-start = ((bf16[8,4,256]{2,1,0:T(4,128)(2,1)}), bf16[8,4,256]{2,1,0:T(4,128)(2,1)S(1)}, u32[]{:S(2)}, u32[]{:S(2)}) async-start(bf16[8,4,256]{2,1,0:T(4,128)(2,1)} %bitcast.1), calls=%async_computation | async-start | bytes 32768 | tf_op jit(solution)/shard_map/all_to_all | solution.py:15
  13.1 32.4 %copy-start.11 = (s32[4]{0:T(128)S(1)}, s32[4]{0:T(128)}, u32[]{:S(2)}) copy-start(s32[4]{0:T(128)} %param.32) | copy-start | bytes 52
  42.2 11.6 %all-to-all-start.2 = ((f32[8,4,1280]{2,1,0:T(4,128)}), f32[8,4,1280]{2,1,0:T(4,128)S(1)}, u32[]{:S(2)}, u32[]{:S(2)}) async-start(f32[8,4,1280]{2,1,0:T(4,128)} %fusion.6), calls=%async_computation.2 | async-start | bytes 327680 | tf_op jit(solution)/shard_map/all_to_all | solution.py:15
  45.6 4.0 %copy-start.8 = (s32[4]{0:T(128)S(1)}, s32[4]{0:T(128)}, u32[]{:S(2)}) copy-start(s32[4]{0:T(128)} %param.21) | copy-start | bytes 52
  49.6 7.8 %copy-start.9 = (f32[3]{0:T(128)S(1)}, f32[3]{0:T(128)}, u32[]{:S(2)}) copy-start(f32[3]{0:T(128)} %param.28) | copy-start | bytes 40
  55.5 2.5 %copy-start.5 = (f32[256]{0:T(256)S(1)}, f32[256]{0:T(256)}, u32[]{:S(2)}) copy-start(f32[256]{0:T(256)} %param.29) | copy-start | bytes 3076
  55.5 6.6 %copy-start.6 = (s32[4,2]{0,1:T(2,128)S(1)}, s32[4,2]{0,1:T(2,128)}, u32[]{:S(2)}) copy-start(s32[4,2]{0,1:T(2,128)} %param.33) | copy-start | bytes 100
  57.2 28.8 %copy-start.1 = (bf16[4,2048]{1,0:T(4,128)(2,1)S(1)}, bf16[4,2048]{1,0:T(4,128)(2,1)}, u32[]{:S(2)}) copy-start(bf16[4,2048]{1,0:T(4,128)(2,1)} %param.20) | copy-start | bytes 49156
  57.2 28.8 %copy-start.2 = (f32[2048]{0:T(1024)S(1)}, f32[2048]{0:T(1024)}, u32[]{:S(2)}) copy-start(f32[2048]{0:T(1024)} %param.24) | copy-start | bytes 24580
  57.2 29.3 %copy-start.3 = (f32[2048]{0:T(1024)S(1)}, f32[2048]{0:T(1024)}, u32[]{:S(2)}) copy-start(f32[2048]{0:T(1024)} %param.31) | copy-start | bytes 24580
  58.7 10.3 %all-to-all-start.3 = ((bf16[8,4,768]{2,1,0:T(4,128)(2,1)}), bf16[8,4,768]{2,1,0:T(4,128)(2,1)S(1)}, u32[]{:S(2)}, u32[]{:S(2)}) async-start(bf16[8,4,768]{2,1,0:T(4,128)(2,1)} %broadcast_in_dim.120), calls=%async_computation.3 | async-start | bytes 98304 | tf_op jit(solution)/shard_map/all_to_all | solution.py:15
  70.0 16.0 %all-to-all-start.4 = ((bf16[16,4,256]{2,1,0:T(4,128)(2,1)}), bf16[16,4,256]{2,1,0:T(4,128)(2,1)S(1)}, u32[]{:S(2)}, u32[]{:S(2)}) async-start(bf16[16,4,256]{2,1,0:T(4,128)(2,1)} %bitcast.20), calls=%async_computation.4 | async-start | bytes 65536 | tf_op jit(solution)/shard_map/all_to_all | solution.py:15
  113.8 10.9 %copy-start.7 = (f32[4,2]{0,1:T(2,128)S(1)}, f32[4,2]{0,1:T(2,128)}, u32[]{:S(2)}) copy-start(f32[4,2]{0,1:T(2,128)} %param.35) | copy-start | bytes 100
  113.8 10.9 %copy-start.10 = (f32[4]{0:T(128)S(1)}, f32[4]{0:T(128)}, u32[]{:S(2)}) copy-start(f32[4]{0:T(128)} %param.34) | copy-start | bytes 52
  116.1 32.7 %copy-start.4 = (f32[1024]{0:T(1024)S(1)}, f32[1024]{0:T(1024)}, u32[]{:S(2)}) copy-start(f32[1024]{0:T(1024)} %param.39) | copy-start | bytes 12292
  117.2 27.6 %all-to-all-start.6 = ((bf16[256,8,128]{2,1,0:T(8,128)(2,1)}), bf16[256,8,128]{2,1,0:T(8,128)(2,1)S(1)}, u32[]{:S(2)}, u32[]{:S(2)}) async-start(bf16[256,8,128]{2,1,0:T(8,128)(2,1)} %reshape.284), calls=%async_computation.6 | async-start | bytes 1048576 | tf_op jit(solution)/shard_map/all_to_all | solution.py:15
where the time goes:
time: 150 us
  blocking collectives  49.9 us (33%)
  waiting for transfers between devices  43.9 us (29%)
  starting transfers between devices  31.8 us (21%)
  matrix products  8.88 us (6%)
  other arithmetic  8 us (5%)
  local copies, waits for them, and re-layouts  6.71 us (4%)
    all_to_all x2, blocking collectives, swap(): return lax.all_to_all(array, axis, 0, 0, tiled=True)  46.9 us
    all_to_all x5, waiting for transfers between devices, swap(): return lax.all_to_all(array, axis, 0, 0, tiled=True)  43.9 us
    all_to_all x5, starting transfers between devices, swap(): return lax.all_to_all(array, axis, 0, 0, tiled=True)  31.8 us
    unnamed x28, local copies, waits for them, and re-layouts  4.09 us
    dot_general x2, matrix products, attend(): jnp.einsum('sghd,scgd->sghc', query_grid[:, :, :, which], cached_keys[:,...  3.14 us
    psum x1, blocking collectives, shards(): lax.psum(jnp.stack((jnp.sum(mixed, 1), jnp.sum(mixed * mixed, 1))), 'tp')  3.04 us
  transfers between devices with their start and end apart: 5, of which 5 were waited for; matrix products, arithmetic and copies ran while one was open for 4% of the time, Pallas kernels for 0%

commit v1 on v0

--- a/solution.py
+++ b/solution.py
@@ -164,7 +164,9 @@
     routed = jnp.sum(combine[:, :, None, None] * both[None], 1).reshape(seqs, half)
     own = lax.dynamic_slice_in_dim(settled, lax.axis_index("tp") * half, half, 1)
     mixed = ALPHA * own.astype(jnp.float32) + routed
-    sums = lax.psum(jnp.stack((jnp.sum(mixed, 1), jnp.sum(mixed * mixed, 1))), "tp")
+    sums = jnp.sum(
+        lax.all_gather(jnp.stack((jnp.sum(mixed, 1), jnp.sum(mixed * mixed, 1))), "tp"), axis=0
+    )
     mean = sums[0] / width
     spread = sums[1] / width - mean * mean
     result = (mixed - mean[:, None]) * lax.rsqrt(spread[:, None] + EPS) * norm2_gain

time: 150 us -> 150 us (level)
    psum x1 -> x0, blocking collectives: 3.04 us -> none  [shards(): lax.psum(jnp.stack((jnp.sum(mixed, 1), jnp.sum(mixed * mixed, 1))), 'tp')]
    all_gather x0 -> x1, blocking collectives: none -> 2.38 us  [shards(): lax.all_gather(jnp.stack((jnp.sum(mixed, 1), jnp.sum(mixed * mixed, 1))),...]
where the time goes in v1:
time: 150 us; the launch traced here: 149 us
  blocking collectives  49.2 us (33%)
  waiting for transfers between devices  43.9 us (29%)
  starting transfers between devices  31.8 us (21%)
  matrix products  8.88 us (6%)
  other arithmetic  8.02 us (5%)
  local copies, waits for them, and re-layouts  6.71 us (4%)
    all_to_all x2, blocking collectives, swap(): return lax.all_to_all(array, axis, 0, 0, tiled=True)  46.9 us
    all_to_all x5, waiting for transfers between devices, swap(): return lax.all_to_all(array, axis, 0, 0, tiled=True)  43.9 us
    all_to_all x5, starting transfers between devices, swap(): return lax.all_to_all(array, axis, 0, 0, tiled=True)  31.8 us
    unnamed x28, local copies, waits for them, and re-layouts  4.09 us
    dot_general x2, matrix products, attend(): jnp.einsum('sghd,scgd->sghc', query_grid[:, :, :, which], cached_keys[:,...  3.14 us
  transfers between devices with their start and end apart: 5, of which 5 were waited for; matrix products, arithmetic and copies ran while one was open for 4% of the time, Pallas kernels for 0%

profile of v1, /device:TPU:1, one launch (start us, length us, event | category | flops | bytes accessed | tf_op | source)
XLA Modules:
  0.0 148.9 jit_solution(13023714836493301443)
XLA Ops:
  0.0 1.0 convert_reduce_fusion.2
  1.0 0.9 fusion.31
  1.9 1.4 fusion.33
  3.3 9.0 %all-to-all-start = ((bf16[8,4,256]{2,1,0:T(4,128)(2,1)}), bf16[8,4,256]{2,1,0:T(4,128)(2,1)S(1)}, u32[]{:S(2)}, u32[]{:S(2)}) async-start(bf16[8,4,256]{2,1,0:T(4,128)(2,1)} %bitcast.1), calls=%async_computation | async-start | bytes 32768 | tf_op jit(solution)/shard_map/all_to_all | solution.py:15
  13.1 5.8 %all-to-all-done = bf16[8,4,256]{2,1,0:T(4,128)(2,1)S(1)} async-done(((bf16[8,4,256]{2,1,0:T(4,128)(2,1)}), bf16[8,4,256]{2,1,0:T(4,128)(2,1)S(1)}, u32[]{:S(2)}, u32[]{:S(2)}) %all-to-all-start) | async-done | bytes 16416 | tf_op jit(solution)/shard_map/all_to_all | solution.py:15
  19.1 22.2 %all_to_all.35 = bf16[16,16,2048]{2,1,0:T(8,128)(2,1)S(1)} all-to-all(bf16[16,16,2048]{2,1,0:T(8,128)(2,1)S(1)} %broadcast_in_dim.116), channel_id=1, replica_groups=mesh['z'=8,'y'=4,'x'=4,'tp'=2] {'y','x'}, dimensions={0} | all-to-all | bytes 2097152 | tf_op jit(solution)/shard_map/all_to_all | solution.py:15
  41.3 0.9 fusion.6
  42.2 3.4 %all-to-all-start.2 = ((f32[8,4,1280]{2,1,0:T(4,128)}), f32[8,4,1280]{2,1,0:T(4,128)S(1)}, u32[]{:S(2)}, u32[]{:S(2)}) async-start(f32[8,4,1280]{2,1,0:T(4,128)} %fusion.6), calls=%async_computation.2 | async-start | bytes 327680 | tf_op jit(solution)/shard_map/all_to_all | solution.py:15
  45.6 4.0 %copy.53 = bf16[4,1024,256]{1,2,0:T(8,128)(2,1)} copy(bf16[4,1024,256]{2,1,0:T(8,128)(2,1)} %param.22) | data formatting | bytes 4194304 | tf_op args[2]
  49.7 4.1 %all-to-all-done.2 = f32[8,4,1280]{2,1,0:T(4,128)S(1)} async-done(((f32[8,4,1280]{2,1,0:T(4,128)}), f32[8,4,1280]{2,1,0:T(4,128)S(1)}, u32[]{:S(2)}, u32[]{:S(2)}) %all-to-all-start.2) | async-done | bytes 163872 | tf_op jit(solution)/shard_map/all_to_all | solution.py:15
  53.9 1.6 %select_reduce_fusion.2 = (f32[4,3]{1,0:T(4,128)S(1)}, f32[4,3,1024]{2,1,0:T(4,128)S(1)}) fusion(pred[4,1024]{1,0:T(4,128)(4,1)S(1)} %iota_compare_fusion, bf16[4,1024,1,2,128]{1,4,3,0,2:T(8,128)(2,1)} %bitcast.113, bf16[4,1,3,1,128]{4,0,3,2,1:T(4,128)(2,1)S(1)} %get-tuple-element.17), kind=kOutput, calls=%fused_computation.34 | convolution fusion | flops 3182580 | bytes 1104944 | tf_op jit(solution)/shard_map/sghd,scgd->sghc/dot_general | solution.py:46
  55.6 1.6 %fusion.21 = (f32[4,3]{1,0:T(4,128)S(1)}, f32[4,3]{1,0:T(4,128)S(1)}, f32[4,3,1024]{2,1,0:T(4,128)S(1)}) fusion(f32[4,3,1024]{2,1,0:T(4,128)S(1)} %get-tuple-element.21, f32[4,3]{1,0:T(4,128)S(1)} %multiply_maximum_fusion.1, pred[4,1024]{1,0:T(4,128)(4,1)S(1)} %iota_compare_fusion, bf16[4,1024,1,2,128]{1,4,3,0,2:T(8,128)(2,1)} %bitcast.114, ...), kind=kOutput, calls=%fused_computation.36 | convolution fusion | flops 3219432 | bytes 1154192 | tf_op jit(solution)/shard_map/sghd,scgd->sghc/dot_general | solution.py:46
  58.7 3.3 %all-to-all-start.3 = ((bf16[8,4,768]{2,1,0:T(4,128)(2,1)}), bf16[8,4,768]{2,1,0:T(4,128)(2,1)S(1)}, u32[]{:S(2)}, u32[]{:S(2)}) async-start(bf16[8,4,768]{2,1,0:T(4,128)(2,1)} %broadcast_in_dim.120), calls=%async_computation.3 | async-start | bytes 98304 | tf_op jit(solution)/shard_map/all_to_all | solution.py:15
  62.1 6.9 %all-to-all-done.3 = bf16[8,4,768]{2,1,0:T(4,128)(2,1)S(1)} async-done(((bf16[8,4,768]{2,1,0:T(4,128)(2,1)}), bf16[8,4,768]{2,1,0:T(4,128)(2,1)S(1)}, u32[]{:S(2)}, u32[]{:S(2)}) %all-to-all-start.3) | async-done | bytes 49184 | tf_op jit(solution)/shard_map/all_to_all | solution.py:15
  70.0 8.5 %all-to-all-start.4 = ((bf16[16,4,256]{2,1,0:T(4,128)(2,1)}), bf16[16,4,256]{2,1,0:T(4,128)(2,1)S(1)}, u32[]{:S(2)}, u32[]{:S(2)}) async-start(bf16[16,4,256]{2,1,0:T(4,128)(2,1)} %bitcast.20), calls=%async_computation.4 | async-start | bytes 65536 | tf_op jit(solution)/shard_map/all_to_all | solution.py:15
  78.7 7.3 %all-to-all-done.4 = bf16[16,4,256]{2,1,0:T(4,128)(2,1)S(1)} async-done(((bf16[16,4,256]{2,1,0:T(4,128)(2,1)}), bf16[16,4,256]{2,1,0:T(4,128)(2,1)S(1)}, u32[]{:S(2)}, u32[]{:S(2)}) %all-to-all-start.4) | async-done | bytes 32800 | tf_op jit(solution)/shard_map/all_to_all | solution.py:15
  86.6 1.0 select_reduce_fusion
  87.6 24.7 %all_to_all.36 = bf16[128,16,128]{2,1,0:T(8,128)(2,1)S(1)} all-to-all(bf16[128,16,128]{2,1,0:T(8,128)(2,1)S(1)} %select_reduce_fusion), channel_id=1, replica_groups=mesh['z'=8,'y'=4,'x'=4,'tp'=2] {'z','y','x'}, dimensions={0} | all-to-all | bytes 1048576 | tf_op jit(solution)/shard_map/all_to_all | solution.py:15
  112.3 1.5 %fusion.4 = f32[128,256]{1,0:T(8,128)S(1)} fusion(bf16[1,2048,256]{2,1,0:T(8,128)(2,1)} %param.36, bf16[16,8,16,128]{3,2,1,0:T(8,128)(2,1)S(1)} %bitcast.109), kind=kOutput, calls=%fused_computation.14 | convolution fusion | flops 134217728 | bytes 1703936 | tf_op jit(solution)/shard_map/dot_general | solution.py:154
  113.8 2.3 %convolution_convert_fusion = bf16[128,2048]{1,0:T(8,128)(2,1)S(1)} fusion(bf16[1,256,2048]{2,1,0:T(8,128)(2,1)} %param.38, bf16[1,2048,256]{2,1,0:T(8,128)(2,1)} %param.37, bf16[16,8,16,128]{3,2,1,0:T(8,128)(2,1)S(1)} %bitcast.110, f32[128,256]{1,0:T(8,128)S(1)} %fusion.4), kind=kOutput, calls=%fused_computation | convolution fusion | flops 268894208 | bytes 3276800 | tf_op jit(solution)/shard_map/dot_general | solution.py:157
  116.2 1.0 reshape.284
  117.2 7.5 %all-to-all-start.6 = ((bf16[256,8,128]{2,1,0:T(8,128)(2,1)}), bf16[256,8,128]{2,1,0:T(8,128)(2,1)S(1)}, u32[]{:S(2)}, u32[]{:S(2)}) async-start(bf16[256,8,128]{2,1,0:T(8,128)(2,1)} %reshape.284), calls=%async_computation.6 | async-start | bytes 1048576 | tf_op jit(solution)/shard_map/all_to_all | solution.py:15
  124.9 19.8 %all-to-all-done.6 = bf16[256,8,128]{2,1,0:T(8,128)(2,1)S(1)} async-done(((bf16[256,8,128]{2,1,0:T(8,128)(2,1)}), bf16[256,8,128]{2,1,0:T(8,128)(2,1)S(1)}, u32[]{:S(2)}, u32[]{:S(2)}) %all-to-all-start.6) | async-done | bytes 524320 | tf_op jit(solution)/shard_map/all_to_all | solution.py:15
  145.8 2.4 %all-gather.1 = f32[2,2,4]{2,1,0:T(2,128)S(1)} all-gather(f32[1,2,4]{2,1,0:T(2,128)S(1)} %maximum_bitcast_fusion), channel_id=2, replica_groups=mesh['z'=8,'y'=4,'x'=4,'tp'=2] {'tp'}, dimensions={0}, use_global_device_ids=true | all-gather | bytes 96 | tf_op jit(solution)/shard_map/all_gather | solution.py:168
  (73 shorter events, 6.4 us)
Async XLA Ops:
  0.0 57.4 %copy-start = (bf16[4,1024,256]{2,1,0:T(8,128)(2,1)S(1)}, bf16[4,1024,256]{2,1,0:T(8,128)(2,1)}, u32[]{:S(2)}) copy-start(bf16[4,1024,256]{2,1,0:T(8,128)(2,1)} %param.23) | copy-start | bytes 6291460
  3.3 15.6 %all-to-all-start = ((bf16[8,4,256]{2,1,0:T(4,128)(2,1)}), bf16[8,4,256]{2,1,0:T(4,128)(2,1)S(1)}, u32[]{:S(2)}, u32[]{:S(2)}) async-start(bf16[8,4,256]{2,1,0:T(4,128)(2,1)} %bitcast.1), calls=%async_computation | async-start | bytes 32768 | tf_op jit(solution)/shard_map/all_to_all | solution.py:15
  13.1 32.4 %copy-start.11 = (s32[4]{0:T(128)S(1)}, s32[4]{0:T(128)}, u32[]{:S(2)}) copy-start(s32[4]{0:T(128)} %param.32) | copy-start | bytes 52
  42.2 11.6 %all-to-all-start.2 = ((f32[8,4,1280]{2,1,0:T(4,128)}), f32[8,4,1280]{2,1,0:T(4,128)S(1)}, u32[]{:S(2)}, u32[]{:S(2)}) async-start(f32[8,4,1280]{2,1,0:T(4,128)} %fusion.6), calls=%async_computation.2 | async-start | bytes 327680 | tf_op jit(solution)/shard_map/all_to_all | solution.py:15
  45.6 4.0 %copy-start.8 = (s32[4]{0:T(128)S(1)}, s32[4]{0:T(128)}, u32[]{:S(2)}) copy-start(s32[4]{0:T(128)} %param.21) | copy-start | bytes 52
  49.6 7.8 %copy-start.9 = (f32[3]{0:T(128)S(1)}, f32[3]{0:T(128)}, u32[]{:S(2)}) copy-start(f32[3]{0:T(128)} %param.28) | copy-start | bytes 40
  55.5 2.5 %copy-start.5 = (f32[256]{0:T(256)S(1)}, f32[256]{0:T(256)}, u32[]{:S(2)}) copy-start(f32[256]{0:T(256)} %param.29) | copy-start | bytes 3076
  55.5 6.6 %copy-start.6 = (s32[4,2]{0,1:T(2,128)S(1)}, s32[4,2]{0,1:T(2,128)}, u32[]{:S(2)}) copy-start(s32[4,2]{0,1:T(2,128)} %param.33) | copy-start | bytes 100
  57.2 28.8 %copy-start.1 = (bf16[4,2048]{1,0:T(4,128)(2,1)S(1)}, bf16[4,2048]{1,0:T(4,128)(2,1)}, u32[]{:S(2)}) copy-start(bf16[4,2048]{1,0:T(4,128)(2,1)} %param.20) | copy-start | bytes 49156
  57.2 28.8 %copy-start.2 = (f32[2048]{0:T(1024)S(1)}, f32[2048]{0:T(1024)}, u32[]{:S(2)}) copy-start(f32[2048]{0:T(1024)} %param.24) | copy-start | bytes 24580
  57.2 29.3 %copy-start.3 = (f32[2048]{0:T(1024)S(1)}, f32[2048]{0:T(1024)}, u32[]{:S(2)}) copy-start(f32[2048]{0:T(1024)} %param.31) | copy-start | bytes 24580
  58.7 10.3 %all-to-all-start.3 = ((bf16[8,4,768]{2,1,0:T(4,128)(2,1)}), bf16[8,4,768]{2,1,0:T(4,128)(2,1)S(1)}, u32[]{:S(2)}, u32[]{:S(2)}) async-start(bf16[8,4,768]{2,1,0:T(4,128)(2,1)} %broadcast_in_dim.120), calls=%async_computation.3 | async-start | bytes 98304 | tf_op jit(solution)/shard_map/all_to_all | solution.py:15
  70.0 16.0 %all-to-all-start.4 = ((bf16[16,4,256]{2,1,0:T(4,128)(2,1)}), bf16[16,4,256]{2,1,0:T(4,128)(2,1)S(1)}, u32[]{:S(2)}, u32[]{:S(2)}) async-start(bf16[16,4,256]{2,1,0:T(4,128)(2,1)} %bitcast.20), calls=%async_computation.4 | async-start | bytes 65536 | tf_op jit(solution)/shard_map/all_to_all | solution.py:15
  113.8 10.9 %copy-start.7 = (f32[4,2]{0,1:T(2,128)S(1)}, f32[4,2]{0,1:T(2,128)}, u32[]{:S(2)}) copy-start(f32[4,2]{0,1:T(2,128)} %param.35) | copy-start | bytes 100
  113.8 10.9 %copy-start.10 = (f32[4]{0:T(128)S(1)}, f32[4]{0:T(128)}, u32[]{:S(2)}) copy-start(f32[4]{0:T(128)} %param.34) | copy-start | bytes 52
  116.1 32.0 %copy-start.4 = (f32[1024]{0:T(1024)S(1)}, f32[1024]{0:T(1024)}, u32[]{:S(2)}) copy-start(f32[1024]{0:T(1024)} %param.39) | copy-start | bytes 12292
  117.2 27.6 %all-to-all-start.6 = ((bf16[256,8,128]{2,1,0:T(8,128)(2,1)}), bf16[256,8,128]{2,1,0:T(8,128)(2,1)S(1)}, u32[]{:S(2)}, u32[]{:S(2)}) async-start(bf16[256,8,128]{2,1,0:T(8,128)(2,1)} %reshape.284), calls=%async_computation.6 | async-start | bytes 1048576 | tf_op jit(solution)/shard_map/all_to_all | solution.py:15
